TPU v7x, 32 devices: a whole 2x2x4 slice. The times are simulated.
32 devices in a mesh: rep: 2 (over x), fs: 8 (over z, y), tp: 2 (over core).
Axes of the slice: x: 2, y: 2, z: 4, core: 2. Of those that a mesh axis runs over, the one named last changes fastest.
Arguments:
- gate_late: bfloat16 [6144, 4096], P(('rep', 'fs'), 'tp'), may hold values from -6 to 6
- up_late: bfloat16 [6144, 4096], P(('rep', 'fs'), 'tp'), may hold values from -6 to 6
- gate_early: bfloat16 [6144, 4096], P(('rep', 'fs'), 'tp'), may hold values from -6 to 6
- up_early: bfloat16 [6144, 4096], P(('rep', 'fs'), 'tp'), may hold values from -6 to 6
- cotangent: bfloat16 [6144, 2048], P(('rep', 'fs')), may hold values from -6 to 6
- w_down: bfloat16 [2048, 4096], P('fs', 'tp'), may hold values from -0.09375 to 0.09375
- grad_in: float32 [2048, 4096], P('fs', 'tp'), may hold values from -6 to 6
Outputs:
- late_out: bfloat16 [6144, 2048], P(('rep', 'fs'))
- gate_grad: bfloat16 [6144, 4096], P(('rep', 'fs'), 'tp')
- up_grad: bfloat16 [6144, 4096], P(('rep', 'fs'), 'tp')
- grad_out: float32 [2048, 4096], P('fs', 'tp')
All inputs are finite; a program needn't handle non-finite values.
Results may differ from a plain program's by a relative error of at most 0.014.
Values may be sent and summed in bfloat16 or wider, within the bound.
A program may use at most 64 MiB of HBM per device.

v0:
```python
import math

import jax
import jax.numpy as jnp
from jax import lax
from jax.sharding import PartitionSpec as P


def per_device(gate_late, up_late, gate_early, up_early, cotangent, w_down, grad_in):
    row_count = gate_late.shape[0]
    hidden_late = (jax.nn.silu(gate_late.astype(jnp.float32)) * up_late.astype(jnp.float32)).astype(
        jnp.bfloat16
    )
    gate_value = gate_early.astype(jnp.float32)
    sigmoid_early = jax.nn.sigmoid(gate_value)
    swish_early = gate_value * sigmoid_early
    up_value = up_early.astype(jnp.float32)
    hidden_early = (swish_early * up_value).astype(jnp.bfloat16)
    partial_value = lax.dot_general(
        hidden_late,
        lax.all_gather(w_down, "fs", axis=0, tiled=True),
        (((1,), (1,)), ((), ())),
        preferred_element_type=jnp.float32,
    )
    columns = cotangent
    hidden_grad = jnp.dot(
        columns,
        lax.all_gather(w_down, "fs", axis=0, tiled=True),
        preferred_element_type=jnp.float32,
    )
    partial_rounded = partial_value.astype(jnp.bfloat16)
    late_out = lax.psum(partial_rounded, "tp").astype(jnp.float32).astype(jnp.bfloat16)
    gate_grad = (
        hidden_grad * up_value * sigmoid_early * (1.0 + gate_value * (1.0 - sigmoid_early))
    ).astype(jnp.bfloat16)
    up_grad = (hidden_grad * swish_early).astype(jnp.bfloat16)
    rep_count = lax.axis_size("rep")
    fs_count = lax.axis_size("fs")
    grad_scale = 1.0 / math.sqrt(row_count * rep_count * fs_count)
    columns = cotangent
    own_rows = lax.psum_scatter(
        lax.dot_general(
            columns, hidden_early, (((0,), (0,)), ((), ())), preferred_element_type=jnp.float32
        ).astype(jnp.bfloat16),
        "fs",
        scatter_dimension=0,
        tiled=True,
    )
    summed = lax.psum(own_rows, "rep").astype(jnp.float32)
    grad_out = grad_in + summed * grad_scale
    return (late_out, gate_grad, up_grad, grad_out)


def solution(mesh):
    placed = (
        P(("rep", "fs"), "tp"),
        P(("rep", "fs"), "tp"),
        P(("rep", "fs"), "tp"),
        P(("rep", "fs"), "tp"),
        P(("rep", "fs"), None),
        P("fs", "tp"),
        P("fs", "tp"),
    )
    return jax.shard_map(
        per_device,
        mesh=mesh,
        in_specs=placed,
        out_specs=(
            P(("rep", "fs"), None),
            P(("rep", "fs"), "tp"),
            P(("rep", "fs"), "tp"),
            P("fs", "tp"),
        ),
        check_vma=False,
    )
```

profile of v0, /device:TPU:0, one launch (start us, length us, event | category | flops | bytes accessed | tf_op | source)
XLA Modules:
  0.0 367.2 jit_solution(3415325175648241326)
XLA Ops:
  7.2 0.0 copy-start
  7.2 0.0 reduce-scatter.2.cloned.1.call-start
  7.2 1.4 copy-done
  8.6 9.1 %convert_bitcast_fusion = bf16[2048,2048]{0,1:T(8,128)(2,1)} fusion(bf16[384,2048]{1,0:T(8,128)(2,1)S(1)} %copy-done, bf16[384,2048]{1,0:T(8,128)(2,1)} %param.10, bf16[384,2048]{1,0:T(8,128)(2,1)} %param.9), kind=kOutput, calls=%fused_computation | convolution fusion | flops 3231711232 | bytes 13107200 | tf_op jit(solution)/shard_map/dot_general | solution.py:42
  17.7 0.0 reduce-scatter.2.cloned.1.call-update
  17.7 0.0 copy-start.1
  17.7 0.0 all-gather.2.cloned.1.call-start
  17.8 0.7 all-gather.2.cloned.1.call-update
  18.5 0.0 all-reduce.5.cloned.1.call-start
  18.5 2.9 copy.11
  21.4 147.0 %reduce-scatter.2.cloned.1.call-done = bf16[256,2048]{0,1:T(8,128)(2,1)} async-done(((bf16[2048,2048]{0,1:T(8,128)(2,1)}), bf16[256,2048]{0,1:T(8,128)(2,1)}) %reduce-scatter.2.cloned.1.call-update) | async-done | bytes 1048592 | tf_op jit(solution)/shard_map/reduce_scatter | solution.py:41
  168.4 0.0 all-reduce.5.cloned.1.call-update
  168.5 0.0 all-reduce.3.cloned.1.call-start
  168.5 125.7 %all-gather.2.cloned.1.call-done = bf16[2048,2048]{1,0:T(8,128)(2,1)} async-done(((bf16[256,2048]{1,0:T(8,128)(2,1)}), bf16[2048,2048]{1,0:T(8,128)(2,1)}) %all-gather.2.cloned.1.call-update) | async-done | bytes 8388624 | tf_op jit(solution)/shard_map/all_gather | solution.py:21
  294.2 0.0 copy-done.1
  294.2 8.7 %convolution_convert_fusion = bf16[384,2048]{1,0:T(8,128)(2,1)} fusion(bf16[2048,2048]{1,0:T(8,128)(2,1)} %all-gather.2.cloned.1.call-done, bf16[384,2048]{1,0:T(8,128)(2,1)S(1)} %copy-done.1, bf16[384,2048]{1,0:T(8,128)(2,1)} %param.7), kind=kOutput, calls=%fused_computation.22 | convolution fusion | flops 3228303360 | bytes 13107200 | tf_op jit(solution)/shard_map/dot_general | solution.py:19
  302.9 0.0 all-reduce.3.cloned.1.call-update
  302.9 9.8 %multiply_convert_fusion = (bf16[384,2048]{1,0:T(8,128)(2,1)}, bf16[384,2048]{1,0:T(8,128)(2,1)}) fusion(bf16[384,2048]{1,0:T(8,128)(2,1)} %param.9, bf16[384,2048]{1,0:T(8,128)(2,1)} %param.10, bf16[384,2048]{1,0:T(8,128)(2,1)S(1)} %copy-done, bf16[2048,2048]{1,0:T(8,128)(2,1)} %all-gather.2.cloned.1.call-done), kind=kOutput, calls=%fused_computation.20 | convolution fusion | flops 3233021952 | bytes 16252928 | tf_op jit(solution)/shard_map/dot_general | solution.py:26
  312.7 22.1 %all-reduce.5.cloned.1.call-done = bf16[256,2048]{0,1:T(8,128)(2,1)} async-done(((bf16[256,2048]{0,1:T(8,128)(2,1)}), bf16[256,2048]{0,1:T(8,128)(2,1)}) %all-reduce.5.cloned.1.call-update) | async-done | bytes 1048592 | tf_op jit(solution)/shard_map/psum | solution.py:49
  334.8 3.4 multiply_add_fusion
  338.2 2.9 copy.12
  341.1 16.8 %all-reduce.3.cloned.1.call-done = bf16[384,2048]{1,0:T(8,128)(2,1)} async-done(((bf16[384,2048]{1,0:T(8,128)(2,1)}), bf16[384,2048]{1,0:T(8,128)(2,1)}) %all-reduce.3.cloned.1.call-update) | async-done | bytes 1572880 | tf_op jit(solution)/shard_map/psum | solution.py:32
  357.9 2.7 copy.15
Async XLA Ops:
  7.2 1.4 copy-start
  7.2 161.2 %reduce-scatter.2.cloned.1.call-start = ((), (), s32[]{:S(2)}) async-start(), calls=%async_computation.3 | async-start | bytes 9437184 | tf_op jit(solution)/shard_map/reduce_scatter | solution.py:41
  17.7 276.5 %copy-start.1 = (bf16[384,2048]{1,0:T(8,128)(2,1)S(1)}, bf16[384,2048]{1,0:T(8,128)(2,1)}, u32[]{:S(2)}) copy-start(bf16[384,2048]{1,0:T(8,128)(2,1)} %param.8) | copy-start | bytes 4718596
  17.7 276.4 %all-gather.2.cloned.1.call-start = ((), (), s32[]{:S(2)}) async-start(), calls=%async_computation.1 | async-start | bytes 9437184 | tf_op jit(solution)/shard_map/all_gather | solution.py:21
  18.5 316.3 %all-reduce.5.cloned.1.call-start = ((), (), s32[]{:S(2)}) async-start(), calls=%async_computation.4 | async-start | bytes 2097152 | tf_op jit(solution)/shard_map/psum | solution.py:49
  168.5 189.5 %all-reduce.3.cloned.1.call-start = ((), (), s32[]{:S(2)}) async-start(), calls=%async_computation.2 | async-start | bytes 3145728 | tf_op jit(solution)/shard_map/psum | solution.py:32
Sparse Core Ops, SparseCore 0:
  17.8 150.5 reduce-scatter.1
  170.6 123.5 all-gather.1
  296.5 38.2 all-reduce.4
  337.5 20.3 all-reduce.2
where the time goes:
time: 367 us
  waiting for transfers between devices  312 us (85%)
  matrix products  27.6 us (8%)
  between operations  13.8 us (4%)
  local copies, waits for them, and re-layouts  9.86 us (3%)
    reduce_scatter x1, waiting for transfers between devices, per_device(): lax.psum_scatter(lax.dot_general(columns, hidden_early, (((0,), (0,)), ((...  147 us
    all_gather x1, waiting for transfers between devices, per_device(): lax.all_gather(w_down, 'fs', axis=0, tiled=True)  126 us
    psum x1, waiting for transfers between devices, per_device(): summed = lax.psum(own_rows, 'rep').astype(jnp.float32)  22.1 us
    psum x1, waiting for transfers between devices, per_device(): lax.psum(partial_rounded, 'tp').astype(jnp.float32).astype(jnp.bfloat16)  16.8 us
    unnamed x7, local copies, waits for them, and re-layouts  9.86 us
    dot_general x1, matrix products, per_device(): jnp.dot(columns, lax.all_gather(w_down, 'fs', axis=0, tiled=True), prefer...  9.75 us
    dot_general x1, matrix products, per_device(): lax.dot_general(columns, hidden_early, (((0,), (0,)), ((), ())), preferre...  9.11 us
    dot_general x1, matrix products, per_device(): lax.dot_general(hidden_late, lax.all_gather(w_down, 'fs', axis=0, tiled=T...  8.72 us
  transfers between devices with their start and end apart: 4, of which 4 were waited for; matrix products, arithmetic and copies ran while one was open for 8% of the time, Pallas kernels for 0%

commit v1 on v0

v1 whole, which is shorter than its diff:
```python
import functools
import math

import jax
import jax.numpy as jnp
from jax import lax
from jax.experimental import pallas as pl
from jax.experimental.pallas import tpu as pltpu
from jax.sharding import PartitionSpec as P

MESH = pl.DeviceIdType.MESH
F32 = jnp.float32
BF16 = jnp.bfloat16
LINK_ROWS = 16


def ring_place(index, count):
    odd = lax.rem(index, 2)
    half = lax.div(index, 2)
    return (1 - odd) * half + odd * (count - 1 - half)


def ring_index(place, count):
    place = lax.rem(place + 2 * count, count)
    back = lax.div(place, count // 2)
    return (1 - back) * 2 * place + back * (2 * (count - 1 - place) + 1)


def kernel(
    n, n_tp, qa, qr, scale,
    gl, ul, ge, ue, cot, cot_t, w, gin,
    late, gg, ug, gout,
    wf, lacc, hg, contrib, rs_s, rs_r, xr_s, xr_r, hl, he, part, fin_s, fin_r,
    ag_ss, ag_rs, xf_ss, xf_rs, rs_ss, rs_rs, xr_ss, xr_rs, fin_ss, fin_rs, tp_ss, tp_rs,
):
    tokens, cols = gl.shape
    rows = w.shape[0]
    half = cols // 2
    rep = lax.axis_index("rep")
    me = lax.axis_index("fs")
    tp = lax.axis_index("tp")
    place = ring_place(me, n)
    right = ring_index(place + 1, n)
    left = ring_index(place + n - 1, n)
    other = 1 - rep

    barrier = pltpu.get_barrier_semaphore()
    for target in (right, left):
        pl.semaphore_signal(barrier, inc=1, device_id={"fs": target}, device_id_type=MESH)
    pl.semaphore_signal(barrier, inc=1, device_id={"rep": other}, device_id_type=MESH)
    for k in range(1, n_tp):
        pl.semaphore_signal(
            barrier, inc=1, device_id={"tp": lax.rem(tp + k, n_tp)}, device_id_type=MESH
        )
    pl.semaphore_wait(barrier, 2 + n_tp)

    lanes = (pl.ds(0, half), pl.ds(half, half))
    towards = (right, left)

    def shard_at(way, step):
        return ring_index(place - step if way == 0 else place + step, n)

    def aligned(value):
        return pl.multiple_of(value, LINK_ROWS)

    ag_rows = pl.ds(aligned(rep * qa), rows - qa)
    ag_mine = pl.ds(aligned(rep * (rows - qa)), qa)
    ag_theirs = pl.ds(aligned(other * (rows - qa)), qa)
    rs_rows = pl.ds(aligned(rep * qr), rows - qr)
    rs_theirs = pl.ds(aligned(other * (rows - qr)), qr)
    rs_within = pl.ds(aligned(rep * (rows - 2 * qr)), qr)

    def gather(way, step, first=False):
        shard = shard_at(way, step)
        spot = wf.at[shard, ag_rows, lanes[way]]
        return pltpu.make_async_remote_copy(
            src_ref=w.at[ag_rows, lanes[way]] if first else spot,
            dst_ref=spot,
            send_sem=ag_ss.at[way, step],
            recv_sem=ag_rs.at[way, step],
            device_id={"fs": towards[way]},
            device_id_type=MESH,
        )

    def gather_wait(way, step):
        spot = wf.at[shard_at(way, step + 1), ag_rows, lanes[way]]
        pltpu.make_async_remote_copy(
            src_ref=spot, dst_ref=spot, send_sem=ag_ss.at[way, step],
            recv_sem=ag_rs.at[way, step], device_id={"fs": towards[way]}, device_id_type=MESH,
        ).wait_recv()

    def cross(way, step, span):
        spot = wf.at[shard_at(way, step + 1), span, lanes[way]]
        return pltpu.make_async_remote_copy(
            src_ref=spot, dst_ref=spot, send_sem=xf_ss.at[way, step],
            recv_sem=xf_rs.at[way, step], device_id={"rep": other}, device_id_type=MESH,
        )

    def reduce_copy(way, step):
        return pltpu.make_async_remote_copy(
            src_ref=rs_s.at[way, step], dst_ref=rs_r.at[way, step],
            send_sem=rs_ss.at[way, step], recv_sem=rs_rs.at[way, step],
            device_id={"fs": towards[way]}, device_id_type=MESH,
        )

    def pair_copy(way, step):
        return pltpu.make_async_remote_copy(
            src_ref=xr_s.at[way, step], dst_ref=xr_r.at[way, step],
            send_sem=xr_ss.at[way, step], recv_sem=xr_rs.at[way, step],
            device_id={"rep": other}, device_id_type=MESH,
        )

    for way in range(2):
        gather(way, 0, first=True).start()

    tile = 16

    @pl.loop(0, tokens // tile)
    def _(i):
        span = pl.ds(pl.multiple_of(i * tile, tile), tile)
        gate = ge[span, :].astype(F32)
        he[span, :] = (gate * (1.0 / (1.0 + jnp.exp(-gate))) * ue[span, :].astype(F32)).astype(BF16)

    def own_share(way, step):
        shard = shard_at(way, step + 1)
        contrib[way] = jnp.dot(cot_t[shard], he[:, lanes[way]], preferred_element_type=F32)
        xr_s[way, step] = contrib[way, rs_theirs, :].astype(BF16)
        pair_copy(way, step).start()

    def running(way, step):
        pair_copy(way, step).wait_recv()
        contrib[way, pl.ds(aligned(rep * (rows - qr)), qr), :] += xr_r[way, step].astype(F32)

    for way in range(2):
        own_share(way, 0)

    @pl.loop(0, tokens // tile)
    def _(i):
        span = pl.ds(pl.multiple_of(i * tile, tile), tile)
        gate = gl[span, :].astype(F32)
        hl[span, :] = (gate * (1.0 / (1.0 + jnp.exp(-gate))) * ul[span, :].astype(F32)).astype(BF16)
        hg[span, :] = jnp.zeros((tile, cols), F32)

    wf[me] = w[...]

    @pl.loop(0, n)
    def _(k):
        lacc[k] = jnp.zeros((tokens, rows), F32)

    for way in range(2):
        running(way, 0)
        rs_s[way, 0] = contrib[way, rs_rows, :].astype(BF16)
        reduce_copy(way, 0).start()

    def use(way, step):
        shard = shard_at(way, step)
        block = wf[shard, :, lanes[way]]
        lacc[shard] += lax.dot_general(
            hl[:, lanes[way]], block, (((1,), (1,)), ((), ())), preferred_element_type=F32
        )
        hg[:, lanes[way]] += jnp.dot(cot[shard], block, preferred_element_type=F32)

    def advance(step, last):
        for way in range(2):
            gather_wait(way, step)
            if not last:
                gather(way, step + 1).start()
            cross(way, step, ag_mine).start()
        for way in range(2):
            own_share(way, step + 1)
        for way in range(2):

            @pl.when(step >= 1)
            def _():
                cross(way, step - 1, ag_theirs).wait_recv()

            use(way, step)
        for way in range(2):
            running(way, step + 1)
            reduce_copy(way, step).wait_recv()
            total = contrib[way, rs_rows, :] + rs_r[way, step].astype(F32)
            if last:
                fin_s[:, lanes[way]] = total.astype(BF16)
            else:
                rs_s[way, step + 1] = total.astype(BF16)
                reduce_copy(way, step + 1).start()

    def body(step, carry):
        advance(step, False)
        return carry

    lax.fori_loop(0, n - 2, body, 0)
    advance(jnp.int32(n - 2), True)

    final = pltpu.make_async_remote_copy(
        src_ref=fin_s, dst_ref=fin_r, send_sem=fin_ss, recv_sem=fin_rs,
        device_id={"rep": other}, device_id_type=MESH,
    )
    final.start()

    for way in range(2):
        cross(way, n - 2, ag_theirs).wait_recv()
        use(way, n - 1)

    @pl.loop(0, n)
    def _(k):
        part[tp, k] = lacc[k].astype(BF16)

    def share(k):
        return pltpu.make_async_remote_copy(
            src_ref=part.at[tp], dst_ref=part.at[tp], send_sem=tp_ss.at[k], recv_sem=tp_rs.at[k],
            device_id={"tp": lax.rem(tp + k, n_tp)}, device_id_type=MESH,
        )

    def share_wait(k):
        spot = part.at[lax.rem(tp + n_tp - k, n_tp)]
        pltpu.make_async_remote_copy(
            src_ref=spot, dst_ref=spot, send_sem=tp_ss.at[k], recv_sem=tp_rs.at[k],
            device_id={"tp": lax.rem(tp + k, n_tp)}, device_id_type=MESH,
        ).wait_recv()

    for k in range(1, n_tp):
        share(k).start()

    @pl.loop(0, tokens // tile)
    def _(i):
        span = pl.ds(pl.multiple_of(i * tile, tile), tile)
        gate = ge[span, :].astype(F32)
        sig = 1.0 / (1.0 + jnp.exp(-gate))
        grad = hg[span, :]
        ug[span, :] = (grad * (gate * sig)).astype(BF16)
        gg[span, :] = (
            grad * ue[span, :].astype(F32) * sig * (1.0 + gate * (1.0 - sig))
        ).astype(BF16)

    for k in range(1, n_tp):
        share_wait(k)

    @pl.loop(0, n)
    def _(k):
        total = part[0, k].astype(F32)
        for j in range(1, n_tp):
            total = total + part[j, k].astype(F32)
        late[k] = total.astype(BF16)

    final.wait_recv()
    shared = rows - 2 * qr
    mine_only = pl.ds(aligned(rep * (rows - qr)), qr)
    theirs_only = pl.ds(aligned(other * (rows - qr)), qr)
    gout[mine_only, :] = gin[mine_only, :] + fin_s[rs_within, :].astype(F32) * scale
    gout[theirs_only, :] = (
        gin[theirs_only, :] + fin_r[pl.ds(aligned(other * shared), qr), :].astype(F32) * scale
    )
    both = pl.ds(qr, shared)
    gout[both, :] = gin[both, :] + scale * (
        fin_s[pl.ds(aligned(other * qr), shared), :].astype(F32)
        + fin_r[pl.ds(aligned(rep * qr), shared), :].astype(F32)
    )

    final.wait_send()
    for k in range(1, n_tp):
        share(k).wait_send()
    for way in range(2):
        gather(way, 0, first=True).wait_send()
        pair_copy(way, n - 1).wait_send()

    @pl.loop(0, n - 1)
    def _(step):
        for way in range(2):
            cross(way, step, ag_mine).wait_send()
            reduce_copy(way, step).wait_send()
            pair_copy(way, step).wait_send()

    @pl.loop(1, n - 1)
    def _(step):
        for way in range(2):
            gather(way, step).wait_send()


def solution(mesh):
    n, n_tp, n_rep = mesh.shape["fs"], mesh.shape["tp"], mesh.shape["rep"]
    assert n_rep == 2 and n % 2 == 0 and n > 2

    def per_device(gl, ul, ge, ue, cotangent, w, gin):
        tokens, cols = gl.shape
        rows, width = w.shape[0], cotangent.shape[1]
        half = cols // 2
        qa = (rows * 5 // 16) // LINK_ROWS * LINK_ROWS
        qr = (rows // 4) // LINK_ROWS * LINK_ROWS
        scale = 1.0 / math.sqrt(tokens * n_rep * n)
        cot = cotangent.reshape(tokens, n, rows).transpose(1, 0, 2)
        cot_t = cotangent.T.reshape(n, rows, tokens)
        vmem = pl.BlockSpec(memory_space=pltpu.VMEM)
        dma = pltpu.SemaphoreType.DMA
        late, gg, ug, gout = pl.pallas_call(
            functools.partial(kernel, n, n_tp, qa, qr, scale),
            out_shape=(
                jax.ShapeDtypeStruct((n, tokens, rows), BF16),
                jax.ShapeDtypeStruct((tokens, cols), BF16),
                jax.ShapeDtypeStruct((tokens, cols), BF16),
                jax.ShapeDtypeStruct((rows, cols), F32),
            ),
            in_specs=[vmem] * 8,
            out_specs=(vmem,) * 4,
            scratch_shapes=[
                pltpu.VMEM((n, rows, cols), BF16),
                pltpu.VMEM((n, tokens, rows), F32),
                pltpu.VMEM((tokens, cols), F32),
                pltpu.VMEM((2, rows, half), F32),
                pltpu.VMEM((2, n - 1, rows - qr, half), BF16),
                pltpu.VMEM((2, n - 1, rows - qr, half), BF16),
                pltpu.VMEM((2, n, qr, half), BF16),
                pltpu.VMEM((2, n, qr, half), BF16),
                pltpu.VMEM((tokens, cols), BF16),
                pltpu.VMEM((tokens, cols), BF16),
                pltpu.VMEM((n_tp, n, tokens, rows), BF16),
                pltpu.VMEM((rows - qr, cols), BF16),
                pltpu.VMEM((rows - qr, cols), BF16),
            ]
            + [dma((2, n))] * 8
            + [dma, dma, dma((n_tp,)), dma((n_tp,))],
            compiler_params=pltpu.CompilerParams(
                collective_id=0, has_side_effects=True, vmem_limit_bytes=67043328
            ),
        )(gl, ul, ge, ue, cot, cot_t, w, gin)
        return late.transpose(1, 0, 2).reshape(tokens, width), gg, ug, gout

    placed = (
        P(("rep", "fs"), "tp"),
        P(("rep", "fs"), "tp"),
        P(("rep", "fs"), "tp"),
        P(("rep", "fs"), "tp"),
        P(("rep", "fs"), None),
        P("fs", "tp"),
        P("fs", "tp"),
    )
    return jax.shard_map(
        per_device,
        mesh=mesh,
        in_specs=placed,
        out_specs=(
            P(("rep", "fs"), None),
            P(("rep", "fs"), "tp"),
            P(("rep", "fs"), "tp"),
            P("fs", "tp"),
        ),
        check_vma=False,
    )
```

time: 367 us -> 164 us (0.45)
  waiting for transfers between devices: 312 us -> 0 us
  Pallas kernels: 0 us -> 149 us
  matrix products: 27.6 us -> 0 us
  between operations: 13.8 us -> 0.68 us
  local copies, waits for them, and re-layouts: 9.86 us -> 14.1 us
    pallas_call x0 -> x1, Pallas kernels: none -> 149 us  [per_device(): pl.pallas_call(functools.partial(kernel, n, n_tp, qa, qr, scale), out_sha...]
    reduce_scatter x1 -> x0, waiting for transfers between devices: 147 us -> none  [per_device(): lax.psum_scatter(lax.dot_general(columns, hidden_early, (((0,), (0,)), ((...]
    all_gather x1 -> x0, waiting for transfers between devices: 126 us -> none  [per_device(): lax.all_gather(w_down, 'fs', axis=0, tiled=True)]
    psum x2 -> x0, waiting for transfers between devices: 38.9 us -> none  [the longest x1 22.1 us: per_device(): summed = lax.psum(own_rows, 'rep').astype(jnp.float32)]
    dot_general x3 -> x0, matrix products: 27.6 us -> none  [the longest x1 9.75 us: per_device(): jnp.dot(columns, lax.all_gather(w_down, 'fs', axis=0, tiled=True), prefer...]
    transpose x0 -> x2, local copies, waits for them, and re-layouts: none -> 4.57 us  [the longest x1 2.7 us: per_device(): cot_t = cotangent.T.reshape(n, rows, tokens)]
    unnamed x7 -> x13, local copies, waits for them, and re-layouts: 9.86 us -> 7.94 us
  transfers between devices with their start and end apart: 4 -> 0, of which waited for: 4 -> 0; matrix products, arithmetic and copies ran while one was open for 8% -> 0% of each run, Pallas kernels for 0% -> 0%
where the time goes in v1:
time: 164 us
  Pallas kernels  149 us (91%)
  local copies, waits for them, and re-layouts  14.1 us (9%)
    pallas_call x1, Pallas kernels, per_device(): pl.pallas_call(functools.partial(kernel, n, n_tp, qa, qr, scale), out_sha...  149 us
    unnamed x13, local copies, waits for them, and re-layouts  7.94 us

profile of v1, /device:TPU:0, one launch (start us, length us, event | category | flops | bytes accessed | tf_op | source)
XLA Modules:
  0.0 164.3 jit_solution(2689148497671613846)
XLA Ops:
  0.6 0.0 copy-start
  0.6 2.7 %copy.14 = bf16[2048,384]{1,0:T(8,128)(2,1)} copy(bf16[2048,384]{0,1:T(8,128)(2,1)} %bitcast.6) | data formatting | bytes 3145728 | tf_op jit(solution)/shard_map/transpose | solution.py:292
  3.3 0.0 copy-done
  3.3 0.9 copy.12
  4.2 1.6 copy.13
  5.8 149.5 %shard_map.102 = (bf16[8,384,256]{2,1,0:T(8,128)(2,1)}, bf16[384,2048]{1,0:T(8,128)(2,1)}, bf16[384,2048]{1,0:T(8,128)(2,1)}, f32[256,2048]{1,0:T(8,128)}) custom-call(bf16[384,2048]{1,0:T(8,128)(2,1)} %gl.1, bf16[384,2048]{1,0:T(8,128)(2,1)} %ul.1, bf16[384,2048]{1,0:T(8,128)(2,1)} %ge.1, bf16[384,2048]{1,0:T(8,128)(2,1)} %ue.1, ...), custom_call_target="tpu_custom_call" | custom-call | tf_op jit(solution)/shard_map/pallas_call | solution.py:295
  155.3 1.9 %copy.15 = bf16[384,8,256]{0,2,1:T(8,128)(2,1)S(1)} copy(bf16[384,8,256]{2,0,1:T(8,128)(2,1)} %bitcast.11) | data formatting | bytes 3145728 | tf_op jit(solution)/shard_map/transpose | solution.py:326
  157.2 0.0 copy-start.3
  157.2 1.6 copy.16
  158.8 0.0 copy-done.3
  158.8 0.0 copy-start.2
  158.8 1.1 copy.20
  160.0 0.8 copy-done.2
  160.8 0.0 copy-start.1
  160.8 1.1 copy.21
  161.9 1.0 copy-done.1
  163.0 1.3 copy.22
Async XLA Ops:
  0.6 2.7 %copy-start = (bf16[384,2048]{1,0:T(8,128)(2,1)S(1)}, bf16[384,2048]{1,0:T(8,128)(2,1)}, u32[]{:S(2)}) copy-start(bf16[384,2048]{1,0:T(8,128)(2,1)} %param.11) | copy-start | bytes 4718596
  157.2 1.6 copy-start.3
  158.8 2.0 %copy-start.2 = (bf16[384,2048]{1,0:T(8,128)(2,1)S(1)}, bf16[384,2048]{1,0:T(8,128)(2,1)}, u32[]{:S(2)}) copy-start(bf16[384,2048]{1,0:T(8,128)(2,1)} %get-tuple-element.22) | copy-start | bytes 4718596
  160.8 2.2 %copy-start.1 = (f32[256,2048]{1,0:T(8,128)S(1)}, f32[256,2048]{1,0:T(8,128)}, u32[]{:S(2)}) copy-start(f32[256,2048]{1,0:T(8,128)} %get-tuple-element.23) | copy-start | bytes 6291460

commit v2 on v1

--- a/solution.py
+++ b/solution.py
@@ -28,7 +28,7 @@
 
 def kernel(
     n, n_tp, qa, qr, scale,
-    gl, ul, ge, ue, cot, cot_t, w, gin,
+    gl, ul, ge, ue, cot, w, gin,
     late, gg, ug, gout,
     wf, lacc, hg, contrib, rs_s, rs_r, xr_s, xr_r, hl, he, part, fin_s, fin_r,
     ag_ss, ag_rs, xf_ss, xf_rs, rs_ss, rs_rs, xr_ss, xr_rs, fin_ss, fin_rs, tp_ss, tp_rs,
@@ -60,6 +60,11 @@
     def shard_at(way, step):
         return ring_index(place - step if way == 0 else place + step, n)
 
+    def columns(ref, shard):
+        if len(ref.shape) == 3:
+            return ref[shard]
+        return ref[:, pl.ds(pl.multiple_of(shard * rows, rows), rows)]
+
     def aligned(value):
         return pl.multiple_of(value, LINK_ROWS)
 
@@ -123,7 +128,10 @@
 
     def own_share(way, step):
         shard = shard_at(way, step + 1)
-        contrib[way] = jnp.dot(cot_t[shard], he[:, lanes[way]], preferred_element_type=F32)
+        contrib[way] = lax.dot_general(
+            columns(cot, shard), he[:, lanes[way]], (((0,), (0,)), ((), ())),
+            preferred_element_type=F32,
+        )
         xr_s[way, step] = contrib[way, rs_theirs, :].astype(BF16)
         pair_copy(way, step).start()
 
@@ -158,23 +166,16 @@
         lacc[shard] += lax.dot_general(
             hl[:, lanes[way]], block, (((1,), (1,)), ((), ())), preferred_element_type=F32
         )
-        hg[:, lanes[way]] += jnp.dot(cot[shard], block, preferred_element_type=F32)
+        hg[:, lanes[way]] += jnp.dot(columns(cot, shard), block, preferred_element_type=F32)
+
+    final = pltpu.make_async_remote_copy(
+        src_ref=fin_s, dst_ref=fin_r, send_sem=fin_ss, recv_sem=fin_rs,
+        device_id={"rep": other}, device_id_type=MESH,
+    )
 
     def advance(step, last):
         for way in range(2):
-            gather_wait(way, step)
-            if not last:
-                gather(way, step + 1).start()
-            cross(way, step, ag_mine).start()
-        for way in range(2):
             own_share(way, step + 1)
-        for way in range(2):
-
-            @pl.when(step >= 1)
-            def _():
-                cross(way, step - 1, ag_theirs).wait_recv()
-
-            use(way, step)
         for way in range(2):
             running(way, step + 1)
             reduce_copy(way, step).wait_recv()
@@ -184,6 +185,20 @@
             else:
                 rs_s[way, step + 1] = total.astype(BF16)
                 reduce_copy(way, step + 1).start()
+        if last:
+            final.start()
+        for way in range(2):
+
+            @pl.when(step >= 1)
+            def _():
+                cross(way, step - 1, ag_theirs).wait_recv()
+
+            use(way, step)
+        for way in range(2):
+            gather_wait(way, step)
+            if not last:
+                gather(way, step + 1).start()
+            cross(way, step, ag_mine).start()
 
     def body(step, carry):
         advance(step, False)
@@ -191,12 +206,6 @@
 
     lax.fori_loop(0, n - 2, body, 0)
     advance(jnp.int32(n - 2), True)
-
-    final = pltpu.make_async_remote_copy(
-        src_ref=fin_s, dst_ref=fin_r, send_sem=fin_ss, recv_sem=fin_rs,
-        device_id={"rep": other}, device_id_type=MESH,
-    )
-    final.start()
 
     for way in range(2):
         cross(way, n - 2, ag_theirs).wait_recv()
@@ -241,7 +250,10 @@
         total = part[0, k].astype(F32)
         for j in range(1, n_tp):
             total = total + part[j, k].astype(F32)
-        late[k] = total.astype(BF16)
+        if len(late.shape) == 3:
+            late[k] = total.astype(BF16)
+        else:
+            late[:, pl.ds(pl.multiple_of(k * rows, rows), rows)] = total.astype(BF16)
 
     final.wait_recv()
     shared = rows - 2 * qr
@@ -251,11 +263,12 @@
     gout[theirs_only, :] = (
         gin[theirs_only, :] + fin_r[pl.ds(aligned(other * shared), qr), :].astype(F32) * scale
     )
-    both = pl.ds(qr, shared)
-    gout[both, :] = gin[both, :] + scale * (
-        fin_s[pl.ds(aligned(other * qr), shared), :].astype(F32)
-        + fin_r[pl.ds(aligned(rep * qr), shared), :].astype(F32)
-    )
+    if shared:
+        both = pl.ds(qr, shared)
+        gout[both, :] = gin[both, :] + scale * (
+            fin_s[pl.ds(aligned(other * qr), shared), :].astype(F32)
+            + fin_r[pl.ds(aligned(rep * qr), shared), :].astype(F32)
+        )
 
     final.wait_send()
     for k in range(1, n_tp):
@@ -285,22 +298,24 @@
         tokens, cols = gl.shape
         rows, width = w.shape[0], cotangent.shape[1]
         half = cols // 2
-        qa = (rows * 5 // 16) // LINK_ROWS * LINK_ROWS
-        qr = (rows // 4) // LINK_ROWS * LINK_ROWS
+        qa = (rows * 3 // 16) // LINK_ROWS * LINK_ROWS
+        qr = (rows * 6 // 16) // LINK_ROWS * LINK_ROWS
         scale = 1.0 / math.sqrt(tokens * n_rep * n)
-        cot = cotangent.reshape(tokens, n, rows).transpose(1, 0, 2)
-        cot_t = cotangent.T.reshape(n, rows, tokens)
+        whole_lanes = rows % 128 == 0
+        cot = cotangent
+        if not whole_lanes:
+            cot = cotangent.reshape(tokens, n, rows).transpose(1, 0, 2)
         vmem = pl.BlockSpec(memory_space=pltpu.VMEM)
         dma = pltpu.SemaphoreType.DMA
         late, gg, ug, gout = pl.pallas_call(
             functools.partial(kernel, n, n_tp, qa, qr, scale),
             out_shape=(
-                jax.ShapeDtypeStruct((n, tokens, rows), BF16),
+                jax.ShapeDtypeStruct(cot.shape, BF16),
                 jax.ShapeDtypeStruct((tokens, cols), BF16),
                 jax.ShapeDtypeStruct((tokens, cols), BF16),
                 jax.ShapeDtypeStruct((rows, cols), F32),
             ),
-            in_specs=[vmem] * 8,
+            in_specs=[vmem] * 7,
             out_specs=(vmem,) * 4,
             scratch_shapes=[
                 pltpu.VMEM((n, rows, cols), BF16),
@@ -322,8 +337,10 @@
             compiler_params=pltpu.CompilerParams(
                 collective_id=0, has_side_effects=True, vmem_limit_bytes=67043328
             ),
-        )(gl, ul, ge, ue, cot, cot_t, w, gin)
-        return late.transpose(1, 0, 2).reshape(tokens, width), gg, ug, gout
+        )(gl, ul, ge, ue, cot, w, gin)
+        if not whole_lanes:
+            late = late.transpose(1, 0, 2).reshape(tokens, width)
+        return late, gg, ug, gout
 
     placed = (
         P(("rep", "fs"), "tp"),

time: 164 us -> 158 us (0.963)
  local copies, waits for them, and re-layouts: 14.1 us -> 8.3 us
    transpose x2 -> x0, local copies, waits for them, and re-layouts: 4.57 us -> none  [the longest x1 2.7 us: per_device(): cot_t = cotangent.T.reshape(n, rows, tokens)]
    unnamed x13 -> x10, local copies, waits for them, and re-layouts: 7.94 us -> 8.3 us
where the time goes in v2:
time: 158 us; the launch traced here: 157 us
  Pallas kernels  148 us (94%)
  local copies, waits for them, and re-layouts  8.3 us (5%)
    pallas_call x1, Pallas kernels, per_device(): pl.pallas_call(functools.partial(kernel, n, n_tp, qa, qr, scale), out_sha...  148 us
    unnamed x10, local copies, waits for them, and re-layouts  8.3 us

profile of v2, /device:TPU:0, one launch (start us, length us, event | category | flops | bytes accessed | tf_op | source)
XLA Modules:
  0.0 157.3 jit_solution(12043335552047940736)
XLA Ops:
  0.6 148.4 %shard_map.102 = (bf16[384,2048]{1,0:T(8,128)(2,1)}, bf16[384,2048]{1,0:T(8,128)(2,1)}, bf16[384,2048]{1,0:T(8,128)(2,1)}, f32[256,2048]{1,0:T(8,128)}) custom-call(bf16[384,2048]{1,0:T(8,128)(2,1)} %gl.1, bf16[384,2048]{1,0:T(8,128)(2,1)} %ul.1, bf16[384,2048]{1,0:T(8,128)(2,1)} %ge.1, bf16[384,2048]{1,0:T(8,128)(2,1)} %ue.1, bf16[384,2048]{1,0:T(8,128)(2,1)} %cot.1, ...), custom_call_target="tpu_custom_call" | custom-call | tf_op jit(solution)/shard_map/pallas_call | solution.py:310
  149.0 0.0 copy-start.2
  149.0 2.8 %copy.15 = bf16[384,2048]{1,0:T(8,128)(2,1)} copy(bf16[384,2048]{1,0:T(8,128)(2,1)} %get-tuple-element.8) | data formatting | bytes 3145728
  151.9 0.0 copy-done.2
  151.9 0.0 copy-start.1
  151.9 1.1 copy.16
  153.0 0.8 copy-done.1
  153.9 0.0 copy-start
  153.9 1.1 copy.17
  155.0 1.0 copy-done
  156.0 1.3 copy.18
Async XLA Ops:
  149.0 2.9 %copy-start.2 = (bf16[384,2048]{1,0:T(8,128)(2,1)S(1)}, bf16[384,2048]{1,0:T(8,128)(2,1)}, u32[]{:S(2)}) copy-start(bf16[384,2048]{1,0:T(8,128)(2,1)} %get-tuple-element.9) | copy-start | bytes 4718596
  151.9 2.0 %copy-start.1 = (bf16[384,2048]{1,0:T(8,128)(2,1)S(1)}, bf16[384,2048]{1,0:T(8,128)(2,1)}, u32[]{:S(2)}) copy-start(bf16[384,2048]{1,0:T(8,128)(2,1)} %get-tuple-element.10) | copy-start | bytes 4718596
  153.9 2.2 %copy-start = (f32[256,2048]{1,0:T(8,128)S(1)}, f32[256,2048]{1,0:T(8,128)}, u32[]{:S(2)}) copy-start(f32[256,2048]{1,0:T(8,128)} %get-tuple-element.11) | copy-start | bytes 6291460
